TPU v7x, 256 devices: a whole 4x4x8 slice. The times are simulated.
256 devices in a mesh: ep: 16 (over y, x), tp: 16 (over z, core).
Axes of the slice: x: 4, y: 4, z: 8, core: 2. Of those that a mesh axis runs over, the one named last changes fastest.
Arguments:
- queries: bfloat16 [32768, 1024], P('ep', 'tp'), may hold values from -600 to 600
- key_rows: bfloat16 [32768, 128], P('ep'), may hold values from -6 to 6
- value_rows: bfloat16 [32768, 128], P('ep'), may hold values from -48 to 48
- sink_logits: float32 [16], P('tp'), may hold values from 2 to 6
- out_weight: bfloat16 [1024, 2048], P('tp'), may hold values from -0.1875 to 0.1875
- moe_rows: bfloat16 [8192, 2048], P(('ep', 'tp')), may hold values from -6 to 6
- moe_gain: float32 [2048], replicated, may hold values from 0.1 to 1.9
- routes: int32 [8192, 2], P(('ep', 'tp')), may hold values from 0 to 15, all different within a row; in each aligned block of 32 rows (0 to 31, 32 to 63, ...) at most 6 rows name the same one
- route_weight: float32 [8192, 2], P(('ep', 'tp')), may hold values from 0.2 to 1
- gate_weight: bfloat16 [16, 2048, 7168], P('ep', None, 'tp'), may hold values from -0.125 to 0.125
- up_weight: bfloat16 [16, 2048, 7168], P('ep', None, 'tp'), may hold values from -0.125 to 0.125
- down_weight: bfloat16 [16, 7168, 2048], P('ep', 'tp'), may hold values from -0.0625 to 0.0625
Outputs:
- mixer_out: bfloat16 [32768, 2048], P(('ep', 'tp'))
- moe_out: bfloat16 [8192, 2048], P(('ep', 'tp'))
Inputs may be any that keep to these rules, and one draw needn't show every extreme that they name: `routes`: in each aligned block of 32 rows (the rows of one device) no expert is named more than 6 times, a bound that some block reaches; each row names 2 different experts.
All inputs are finite; a program needn't handle non-finite values.
Results may differ from a plain program's by a relative error of at most 0.02.
Values may be sent and summed in bfloat16 or wider, within the bound.
A program may use at most 128 MiB of HBM per device.

v0:
```python
import jax
import jax.numpy as jnp
from jax import lax
from jax.sharding import Mesh
from jax.sharding import PartitionSpec as P

HEADS = 16
KV_HEADS = 2
HEAD_DIM = 64
WINDOW = 128
TOP = 2
TP = ("tp_0", "tp_1")
EP_TP = ("ep", "tp_0", "tp_1")


big_negative = -1e30
norm_eps = 1e-05


def passed_along(value, axis, steps):
    count = lax.axis_size(axis)
    initial, last = (max(0, -steps), min(count, count - steps))
    return lax.ppermute(value, axis, [(source, source + steps) for source in range(initial, last)])


def own_block(blocks, axes, order):
    inside = blocks.shape[1:]
    blocks = blocks.reshape(*(lax.axis_size(a) for a in axes), *inside)
    blocks = jnp.moveaxis(blocks, order, range(len(axes))).reshape(-1, *inside)
    for k in order:
        blocks = lax.psum_scatter(blocks, axes[k], scatter_dimension=0, tiled=True)
    return blocks[0]


def split_up(x, dim, devices):
    before, after = (x.shape[:dim], x.shape[dim + 1 :])
    return jnp.moveaxis(x.reshape(*before, devices, -1, *after), dim, 0)


def summed_rows(x, axes, order, dim):
    devices = lax.axis_size(axes)
    return own_block(split_up(x, dim, devices), axes, order)


def layer_normed(inputs, gain):
    values = inputs.astype(jnp.float32)
    center = values - jnp.mean(values, -1, keepdims=True)
    spread = jnp.mean(center * center, -1, keepdims=True)
    return (center * lax.rsqrt(spread + norm_eps) * gain).astype(jnp.bfloat16)


def attend(queries, key_rows, value_rows, sink_logits):
    total = queries.shape[0]
    heads_here = sink_logits.shape[0]
    blocks = total // WINDOW
    key_head = lax.axis_index(TP) * heads_here // (HEADS // KV_HEADS)
    key_own = lax.dynamic_slice_in_dim(key_rows, key_head * HEAD_DIM, HEAD_DIM, 1)
    value_own = lax.dynamic_slice_in_dim(value_rows, key_head * HEAD_DIM, HEAD_DIM, 1)
    last_rows = jnp.concatenate([key_own[total - WINDOW :], value_own[total - WINDOW :]], 1)
    earlier = passed_along(last_rows, "ep", 1)
    key_ext = jnp.concatenate([earlier[:, :HEAD_DIM], key_own], 0)
    value_ext = jnp.concatenate([earlier[:, HEAD_DIM:], value_own], 0)
    key_blocks = jnp.concatenate(
        [
            key_ext[:total].reshape(blocks, WINDOW, HEAD_DIM),
            key_ext[WINDOW:].reshape(blocks, WINDOW, HEAD_DIM),
        ],
        1,
    )
    value_blocks = jnp.concatenate(
        [
            value_ext[:total].reshape(blocks, WINDOW, HEAD_DIM),
            value_ext[WINDOW:].reshape(blocks, WINDOW, HEAD_DIM),
        ],
        1,
    )
    query_blocks = queries.reshape(blocks, WINDOW, heads_here, HEAD_DIM)
    scores = jnp.einsum(
        "nqhd,nkd->nhqk", query_blocks, key_blocks, preferred_element_type=jnp.float32
    ) * HEAD_DIM ** (-0.5)
    anchor = lax.axis_index("ep") * total
    block_base = anchor + jnp.arange(blocks, dtype=jnp.int32)[:, None, None] * WINDOW
    query_pos = block_base + jnp.arange(WINDOW, dtype=jnp.int32)[None, :, None]
    key_pos = block_base - WINDOW + jnp.arange(2 * WINDOW, dtype=jnp.int32)[None, None, :]
    allowed = ((key_pos <= query_pos) & (key_pos > query_pos - WINDOW) & (key_pos >= 0))[:, None]
    masked = jnp.where(allowed, scores, big_negative)
    sinks = sink_logits[None, :, None]
    row_max = jnp.maximum(jnp.max(masked, -1), sinks)
    powers = jnp.where(allowed, jnp.exp(masked - row_max[..., None]), 0.0)
    totals = jnp.sum(powers, -1) + jnp.exp(sinks - row_max)
    attn_probs = (powers / totals[..., None]).astype(jnp.bfloat16)
    attended = jnp.einsum(
        "nhqk,nkd->nqhd", attn_probs, value_blocks, preferred_element_type=jnp.float32
    )
    return attended.astype(jnp.bfloat16).reshape(total, heads_here * HEAD_DIM)


def mixer(queries, key_rows, value_rows, sink_logits, out_weight):
    attended = attend(queries, key_rows, value_rows, sink_logits)
    summed = summed_rows(
        jnp.dot(attended, out_weight, preferred_element_type=jnp.float32).astype(jnp.bfloat16),
        TP,
        (1, 0),
        0,
    ).astype(jnp.float32)
    return summed.astype(jnp.bfloat16)


def experts(moe_rows, moe_gain, routes, route_weight, gate_weight, up_weight, down_weight):
    row_count = moe_rows.shape[0]
    width_all = moe_rows.shape[1]
    expert_count = gate_weight.shape[0] * lax.axis_size("ep")
    capacity = 3 * row_count * TOP // (2 * expert_count)
    normed = layer_normed(moe_rows, moe_gain)
    chosen = routes.reshape(-1)
    onehot = (chosen[:, None] == jnp.arange(expert_count, dtype=jnp.int32)[None, :]).astype(
        jnp.int32
    )
    earlier_count = jnp.cumsum(onehot, 0) - onehot
    slot_index = jnp.sum(earlier_count * onehot, 1)
    target = chosen * capacity + slot_index
    matches = target[None, :] == jnp.arange(expert_count * capacity, dtype=jnp.int32)[:, None]
    dispatch_map = jnp.sum(matches.reshape(expert_count * capacity, row_count, TOP), -1).astype(
        jnp.bfloat16
    )
    buffer = jnp.dot(dispatch_map, normed, preferred_element_type=jnp.float32).astype(jnp.bfloat16)
    buffer = buffer.reshape(expert_count, capacity, width_all)
    gate_mat = gate_weight[0]
    up_mat = up_weight[0]
    down_mat = down_weight[0]
    received = lax.all_to_all(buffer, "ep", split_axis=0, concat_axis=0, tiled=True)
    total = received.shape[0] * received.shape[1]
    flat_rows = received.reshape(total, width_all)
    shard_rows = lax.all_gather(flat_rows, TP, axis=0, tiled=True)
    gate_val = jnp.dot(shard_rows, gate_mat, preferred_element_type=jnp.float32)
    up_val = jnp.dot(shard_rows, up_mat, preferred_element_type=jnp.float32)
    hidden = (jax.nn.silu(gate_val) * up_val).astype(jnp.bfloat16)
    summed = lax.psum_scatter(
        jnp.dot(hidden, down_mat, preferred_element_type=jnp.float32).astype(jnp.bfloat16),
        TP,
        scatter_dimension=0,
        tiled=True,
    )
    results = summed.reshape(received.shape)
    returned = lax.all_to_all(results, "ep", split_axis=0, concat_axis=0, tiled=True)
    weights_flat = route_weight.reshape(-1)
    combine_map = jnp.sum(
        jnp.where(matches, weights_flat[None, :], 0.0).reshape(
            expert_count * capacity, row_count, TOP
        ),
        -1,
    )
    returned_flat = returned.reshape(expert_count * capacity, width_all).astype(jnp.float32)
    moe_out = lax.dot_general(
        combine_map, returned_flat, (((0,), (0,)), ((), ())), precision=lax.Precision.HIGHEST
    )
    return moe_out.astype(jnp.bfloat16)


def body(
    queries,
    key_rows,
    value_rows,
    sink_logits,
    out_weight,
    moe_rows,
    moe_gain,
    routes,
    route_weight,
    gate_weight,
    up_weight,
    down_weight,
):
    mixer_out = mixer(queries, key_rows, value_rows, sink_logits, out_weight)
    moe_out = experts(moe_rows, moe_gain, routes, route_weight, gate_weight, up_weight, down_weight)
    return (mixer_out, moe_out)


def solution(mesh):
    split = Mesh(mesh.devices.reshape(mesh.shape["ep"], 8, 2), ("ep", "tp_0", "tp_1"))
    in_specs = (
        P("ep", TP),
        P("ep", None),
        P("ep", None),
        P(TP),
        P(TP, None),
        P(EP_TP, None),
        P(),
        P(EP_TP, None),
        P(EP_TP, None),
        P("ep", None, TP),
        P("ep", None, TP),
        P("ep", TP, None),
    )
    out_specs = (P(EP_TP, None), P(EP_TP, None))
    return jax.shard_map(body, mesh=split, in_specs=in_specs, out_specs=out_specs, check_vma=False)
```

profile of v0, /device:TPU:1, one launch (start us, length us, event | category | flops | bytes accessed | tf_op | source)
XLA Modules:
  0.0 234.1 jit_solution(17342705961837728711)
XLA Ops:
  8.0 0.0 copy-start
  8.0 0.0 all-gather.2.cloned.1.call-start
  8.1 0.9 copy.65
  8.9 0.1 eq.30
  9.0 0.1 fusion.31
  9.1 0.1 reduce_window_sum.11
  9.2 0.2 select_reduce_fusion.1
  9.4 0.1 reduce_sum.58
  9.5 0.1 copy.66
  9.6 0.7 multiply_add_fusion
  10.3 0.1 convert_reduce_fusion.1
  10.4 0.0 copy-start.1
  10.4 1.1 convert_reduce_fusion
  11.5 1.1 fusion.20
  12.6 1.2 convolution_convert_fusion.2
  13.8 0.1 reshape.236
  14.0 17.8 %all_to_all.10 = bf16[16,6,2048]{2,1,0:T(8,128)(2,1)S(1)} all-to-all(bf16[16,6,2048]{2,1,0:T(8,128)(2,1)S(1)} %reshape.236), channel_id=1, replica_groups=mesh['ep'=16,'tp_0'=8,'tp_1'=2] {'ep'}, dimensions={0} | all-to-all | bytes 786432 | tf_op jit(solution)/shard_map/all_to_all | solution.py:131
  31.8 0.9 reshape.237
  32.7 0.0 all-gather.2.cloned.1.call-update
  32.7 0.0 reduce-scatter.4.cloned.1.call-start
  32.8 0.8 dynamic-slice
  33.6 0.0 copy-done.1
  33.6 0.1 dynamic-slice.1
  33.7 0.1 pad_maximum_fusion.2
  33.8 2.2 collective-permute-start
  36.0 0.1 iota_add_fusion.1
  36.1 0.1 iota_add_fusion
  36.2 1.4 constant_dynamic-slice_fusion
  37.6 0.1 broadcast_compare_fusion
  37.7 0.9 copy.60
  39.2 0.9 copy.56
  40.1 0.0 collective-permute-done
  40.1 0.1 fusion.39
  40.2 0.1 pad_maximum_fusion
  40.3 0.2 copy.59
  40.5 0.1 pad_maximum_fusion.1
  40.6 0.2 copy.55
  40.9 2.6 %fusion.1 = (f32[16,128]{1,0:T(8,128)S(1)}, f32[16,256,128]{2,1,0:T(8,128)S(1)}) fusion(pred[16,256]{1,0:T(8,128)(4,1)S(1)} %broadcast_compare_fusion, s32[16,128]{1,0:T(8,128)S(1)} %get-tuple-element.5, s32[16,128]{1,0:T(8,128)S(1)} %get-tuple-element.4, s32[16,256]{1,0:T(8,128)S(1)} %iota_add_fusion, bf16[16,128,64]{1,2,0:T(8,128)(2,1)} %copy.60, ...), kind=kOutput, calls=%fused_computation.10 | convolution fusion | flops 71825408 | bytes 2928640 | tf_op jit(solution)/shard_map/nqhd,nkd->nhqk/dot_general | solution.py:78
  43.5 1.5 fusion.6
  45.0 0.0 copy-done.3
  45.1 0.0 copy-start.2
  45.1 2.9 %fusion.7 = bf16[16,128,1,64]{1,3,0,2:T(8,128)(2,1)S(1)} fusion(f32[16,256,128]{2,1,0:T(8,128)S(1)} %get-tuple-element.7, f32[16,128]{1,0:T(8,128)S(1)} %exponential_add_fusion, f32[16,128]{1,0:T(8,128)S(1)} %broadcast_maximum_fusion, bf16[16,128,64]{1,2,0:T(8,128)(2,1)S(1)} %copy-done.3, bf16[16,128,64]{1,2,0:T(8,128)(2,1)S(1)} %copy.55, ...), kind=kOutput, calls=%fused_computation.17 | convolution fusion | flops 73531392 | bytes 2936832 | tf_op jit(solution)/shard_map/nhqk,nkd->nqhd/dot_general | solution.py:92
  48.0 0.2 copy.63
  48.2 5.7 %convolution_convert_fusion.1 = bf16[2048,2048]{1,0:T(8,128)(2,1)} fusion(bf16[64,2048]{1,0:T(8,128)(2,1)S(1)} %copy-done.2, bf16[8,8,16,128]{3,2,1,0:T(8,128)(2,1)S(1)} %bitcast.72), kind=kOutput, calls=%fused_computation.1 | convolution fusion | flops 541065216 | bytes 8912896 | tf_op jit(solution)/shard_map/dot_general | solution.py:101
  53.9 8.5 %copy.64 = bf16[2,8,128,2048]{3,2,1,0:T(8,128)(2,1)} copy(bf16[2,8,128,2048]{3,2,0,1:T(8,128)(2,1)} %bitcast.66) | data formatting | bytes 16777216 | tf_op jit(solution)/shard_map/transpose | solution.py:29
  62.5 0.0 reduce-scatter.4.cloned.1.call-update
  62.5 0.2 reduce-scatter.8.cloned.1.call-start
  62.7 17.0 %all-gather.2.cloned.1.call-done = bf16[1536,2048]{1,0:T(8,128)(2,1)} async-done(((bf16[96,2048]{1,0:T(8,128)(2,1)}), bf16[1536,2048]{1,0:T(8,128)(2,1)}) %all-gather.2.cloned.1.call-update) | async-done | bytes 6291472 | tf_op jit(solution)/shard_map/all_gather | solution.py:134
  79.8 10.0 %fusion.4 = f32[1536,448]{0,1:T(8,128)} fusion(bf16[1536,2048]{1,0:T(8,128)(2,1)} %all-gather.2.cloned.1.call-done, bf16[1,2048,448]{1,2,0:T(8,128)(2,1)} %param.21), kind=kOutput, calls=%fused_computation.13 | convolution fusion | flops 2818572288 | bytes 10878976 | tf_op jit(solution)/shard_map/dot_general | solution.py:135
  89.7 0.0 copy-done
  89.8 13.2 %convolution_convert_fusion = bf16[1536,2048]{1,0:T(8,128)(2,1)} fusion(bf16[1,448,2048]{2,1,0:T(8,128)(2,1)S(1)} %copy-done, bf16[1536,2048]{1,0:T(8,128)(2,1)} %all-gather.2.cloned.1.call-done, f32[1536,448]{0,1:T(8,128)} %fusion.4, bf16[1,2048,448]{1,2,0:T(8,128)(2,1)} %param.22), kind=kOutput, calls=%fused_computation | convolution fusion | flops 5644419072 | bytes 19005440 | tf_op jit(solution)/shard_map/dot_general | solution.py:139
  102.9 0.0 reduce-scatter.8.cloned.1.call-update
  103.0 0.0 reduce-scatter.6.cloned.1.call-start
  103.0 0.0 reduce-scatter.4.cloned.1.call-done
  103.0 0.0 copy-start.4
  103.1 0.5 reduce-scatter.6.cloned.1.call-update
  103.5 63.1 %reduce-scatter.8.cloned.1.call-done = bf16[96,2048]{1,0:T(8,128)(2,1)} async-done(((bf16[1536,2048]{1,0:T(8,128)(2,1)}), bf16[96,2048]{1,0:T(8,128)(2,1)}) %reduce-scatter.8.cloned.1.call-update) | async-done | bytes 393232 | tf_op jit(solution)/shard_map/reduce_scatter | solution.py:138
  166.7 1.9 reshape.238
  168.6 6.5 %all-to-all-start.1 = ((bf16[16,6,2048]{2,1,0:T(8,128)(2,1)}), bf16[16,6,2048]{2,1,0:T(8,128)(2,1)S(1)}, u32[]{:S(2)}, u32[]{:S(2)}) async-start(bf16[16,6,2048]{2,1,0:T(8,128)(2,1)} %reshape.238), calls=%async_computation.4 | async-start | bytes 1048576 | tf_op jit(solution)/shard_map/all_to_all | solution.py:145
  175.1 0.1 select_reduce_fusion
  175.2 9.0 %all-to-all-done.1 = bf16[16,6,2048]{2,1,0:T(8,128)(2,1)S(1)} async-done(((bf16[16,6,2048]{2,1,0:T(8,128)(2,1)}), bf16[16,6,2048]{2,1,0:T(8,128)(2,1)S(1)}, u32[]{:S(2)}, u32[]{:S(2)}) %all-to-all-start.1) | async-done | bytes 393248 | tf_op jit(solution)/shard_map/all_to_all | solution.py:145
  184.1 0.1 reshape.239
  184.3 0.9 convolution_convert_fusion.3
  185.2 41.3 %reduce-scatter.6.cloned.1.call-done = bf16[1,128,2048]{2,1,0:T(8,128)(2,1)} async-done(((bf16[8,128,2048]{2,1,0:T(8,128)(2,1)}), bf16[1,128,2048]{2,1,0:T(8,128)(2,1)}) %reduce-scatter.6.cloned.1.call-update) | async-done | bytes 524304 | tf_op jit(solution)/shard_map/reduce_scatter | solution.py:31
  (8 shorter events, 0.0 us)
Async XLA Ops:
  8.0 81.8 %copy-start = (bf16[1,448,2048]{2,1,0:T(8,128)(2,1)S(1)}, bf16[1,448,2048]{2,1,0:T(8,128)(2,1)}, u32[]{:S(2)}) copy-start(bf16[1,448,2048]{2,1,0:T(8,128)(2,1)} %param.23) | copy-start | bytes 5505028
  8.0 71.7 %all-gather.2.cloned.1.call-start = ((), (), s32[]{:S(2)}) async-start(), calls=%async_computation.7 | async-start | bytes 6684672 | tf_op jit(solution)/shard_map/all_gather | solution.py:134
  10.4 23.2 %copy-start.1 = (bf16[2048,128]{1,0:T(8,128)(2,1)S(1)}, bf16[2048,128]{1,0:T(8,128)(2,1)}, u32[]{:S(2)}) copy-start(bf16[2048,128]{1,0:T(8,128)(2,1)} %param.14) | copy-start | bytes 1572868
  32.7 70.4 %reduce-scatter.4.cloned.1.call-start = ((), (), s32[]{:S(2)}) async-start(), calls=%async_computation.5 | async-start | bytes 12582912 | tf_op jit(solution)/shard_map/reduce_scatter | solution.py:31
  33.8 6.3 %collective-permute-start = (bf16[128,128]{1,0:T(8,128)(2,1)S(1)}, bf16[128,128]{1,0:T(8,128)(2,1)S(1)}, u32[]{:S(2)}, u32[]{:S(2)}) collective-permute-start(bf16[128,128]{1,0:T(8,128)(2,1)S(1)} %pad_maximum_fusion.2), channel_id=1, source_target_pairs={{0,16},{16,32},{32,48},{48,64},{64,80},{80,96},{96,112},{112,128},... | collective-permute-start | bytes 98312 | tf_op jit(solution)/shard_map/ppermute | solution.py:23
  43.5 1.6 copy-start.3
  45.1 3.1 %copy-start.2 = (bf16[64,2048]{1,0:T(8,128)(2,1)S(1)}, bf16[64,2048]{1,0:T(8,128)(2,1)}, u32[]{:S(2)}) copy-start(bf16[64,2048]{1,0:T(8,128)(2,1)} %param.16) | copy-start | bytes 786436
  62.5 104.2 %reduce-scatter.8.cloned.1.call-start = ((), (), s32[]{:S(2)}) async-start(), calls=%async_computation.8 | async-start | bytes 6684672 | tf_op jit(solution)/shard_map/reduce_scatter | solution.py:138
  103.0 123.5 %reduce-scatter.6.cloned.1.call-start = ((), (), s32[]{:S(2)}) async-start(), calls=%async_computation.6 | async-start | bytes 4718592 | tf_op jit(solution)/shard_map/reduce_scatter | solution.py:31
  103.0 72.0 %copy-start.4 = (f32[32,2]{0,1:T(2,128)S(1)}, f32[32,2]{0,1:T(2,128)}, u32[]{:S(2)}) copy-start(f32[32,2]{0,1:T(2,128)} %param.20) | copy-start | bytes 772
  168.6 15.6 %all-to-all-start.1 = ((bf16[16,6,2048]{2,1,0:T(8,128)(2,1)}), bf16[16,6,2048]{2,1,0:T(8,128)(2,1)S(1)}, u32[]{:S(2)}, u32[]{:S(2)}) async-start(bf16[16,6,2048]{2,1,0:T(8,128)(2,1)} %reshape.238), calls=%async_computation.4 | async-start | bytes 1048576 | tf_op jit(solution)/shard_map/all_to_all | solution.py:145
Sparse Core Ops, SparseCore 0:
  32.8 46.9 all-gather.1
Sparse Core Ops, SparseCore 1:
  62.6 25.4 reduce-scatter.3
  103.0 63.5 reduce-scatter.7
  169.6 56.8 reduce-scatter.5
where the time goes:
time: 235 us; the launch traced here: 234 us
  waiting for transfers between devices  131 us (56%)
  matrix products  36.6 us (16%)
  blocking collectives  17.8 us (8%)
  local copies, waits for them, and re-layouts  17.6 us (7%)
  between operations  16.6 us (7%)
  starting transfers between devices  9.03 us (4%)
  other arithmetic  5.48 us (2%)
    reduce_scatter x1, waiting for transfers between devices, experts(): lax.psum_scatter(jnp.dot(hidden, down_mat, preferred_element_type=jnp.flo...  63.1 us
    reduce_scatter x2, waiting for transfers between devices, own_block(): blocks = lax.psum_scatter(blocks, axes[k], scatter_dimension=0, tiled=True)  41.3 us
    all_to_all x1, blocking collectives, experts(): lax.all_to_all(buffer, 'ep', split_axis=0, concat_axis=0, tiled=True)  17.8 us
    all_gather x1, waiting for transfers between devices, experts(): shard_rows = lax.all_gather(flat_rows, TP, axis=0, tiled=True)  17 us
    dot_general x1, matrix products, experts(): jnp.dot(hidden, down_mat, preferred_element_type=jnp.float32)  13.2 us
    dot_general x1, matrix products, experts(): gate_val = jnp.dot(shard_rows, gate_mat, preferred_element_type=jnp.float32)  9.99 us
    all_to_all x1, waiting for transfers between devices, experts(): lax.all_to_all(results, 'ep', split_axis=0, concat_axis=0, tiled=True)  8.98 us
    transpose x1, local copies, waits for them, and re-layouts, own_block(): blocks = jnp.moveaxis(blocks, order, range(len(axes))).reshape(-1, *inside)  8.52 us
  transfers between devices with their start and end apart: 6, of which 4 were waited for; matrix products, arithmetic and copies ran while one was open for 23% of the time, Pallas kernels for 0%

commit v1 on v0

v1 whole, which is shorter than its diff:
```python
import jax
import jax.numpy as jnp
from jax import lax
from jax.experimental import pallas as pl
from jax.experimental.pallas import tpu as pltpu
from jax.sharding import PartitionSpec as P

MESH = pl.DeviceIdType.MESH
F32 = jnp.float32
BF16 = jnp.bfloat16
HEAD_DIM = 64
WINDOW = 128
NORM_EPS = 1e-5
EP = 16
NZ = 8
TPN = 16
CAP = 6
ROWS = 96
HALF = 48
D = 2048
FF = 448
LONG = ((4, 3), (3, 4))


def nt(a, b):
    return lax.dot_general(a, b, (((1,), (1,)), ((), ())), preferred_element_type=F32)


def mm(a, b):
    return jnp.dot(a, b, preferred_element_type=F32)


def iota(shape, dim):
    return lax.broadcasted_iota(jnp.int32, shape, dim)


def wrap(i, n):
    return lax.rem(i + n, n)


def kernel(
    rows_ref,
    gain_ref,
    routes_ref,
    rw_ref,
    sink_ref,
    q_hbm,
    k_hbm,
    v_hbm,
    ow_hbm,
    wg_hbm,
    wu_hbm,
    wd_hbm,
    mix_ref,
    moe_ref,
    wg,
    wu,
    wd,
    qv,
    qsend,
    qrecv,
    sksend,
    skrecv,
    kbuf,
    vbuf,
    kz,
    vz,
    att,
    wr,
    asend,
    arecv,
    agbuf,
    pbuf,
    outbox,
    inbox,
    rs_send,
    rs_recv,
    bsend,
    brecv,
    loc,
    s_a,
    r_a,
    s_b,
    r_b,
    s_q,
    r_q,
    s_k,
    r_k,
    s_h,
    r_h,
    s_wz,
    r_wz,
    s_wp,
    r_wp,
    s_wd,
    r_wd,
    s_ag,
    r_ag,
    s_d,
    r_d,
    s_x,
    r_x,
    s_rs,
    r_rs,
):
    e = lax.axis_index("ep")
    t = lax.axis_index("tp")
    z = t // 2
    c = lax.rem(t, 2)
    right = (e, wrap(z + 1, NZ) * 2 + c)
    left = (e, wrap(z - 1, NZ) * 2 + c)
    partner = (e, z * 2 + 1 - c)
    ring = (right, left)

    def rcopy(src, dst, ss, rs, dev):
        return pltpu.make_async_remote_copy(
            src_ref=src, dst_ref=dst, send_sem=ss, recv_sem=rs, device_id=dev, device_id_type=MESH
        )

    def each(lo, hi, fn):
        def body(j, carry):
            fn(j)
            return carry

        lax.fori_loop(lo, hi, body, 0)

    barrier = pltpu.get_barrier_semaphore()

    def greet(j):
        pl.semaphore_signal(barrier, inc=1, device_id=(wrap(e + j, EP), t), device_id_type=MESH)
        pl.semaphore_signal(barrier, inc=1, device_id=(e, wrap(t + j, TPN)), device_id_type=MESH)

    each(1, EP, greet)

    prev = jnp.maximum(t - 1, 0) * WINDOW
    prev = pl.multiple_of(prev, WINDOW)
    own = pl.multiple_of(t * WINDOW, WINDOW)
    wcol = pl.multiple_of(e * 128, 128)
    zrow = pl.multiple_of(z * HEAD_DIM, HEAD_DIM)
    local = [
        pltpu.make_async_copy(q_hbm, qv, loc.at[0]),
        pltpu.make_async_copy(
            ow_hbm.at[:, pl.ds(wcol, 128)], wr.at[c, e, pl.ds(zrow, HEAD_DIM)], loc.at[1]
        ),
        pltpu.make_async_copy(k_hbm.at[pl.ds(prev, WINDOW)], kbuf.at[0], loc.at[2]),
        pltpu.make_async_copy(k_hbm.at[pl.ds(own, WINDOW)], kbuf.at[1], loc.at[3]),
        pltpu.make_async_copy(v_hbm.at[pl.ds(prev, WINDOW)], vbuf.at[0], loc.at[4]),
        pltpu.make_async_copy(v_hbm.at[pl.ds(own, WINDOW)], vbuf.at[1], loc.at[5]),
        pltpu.make_async_copy(wg_hbm.at[0], wg, loc.at[6]),
        pltpu.make_async_copy(wu_hbm.at[0], wu, loc.at[7]),
        pltpu.make_async_copy(wd_hbm.at[0], wd, loc.at[8]),
    ]
    for cp in local:
        cp.start()

    values = rows_ref[...].astype(F32)
    center = values - jnp.mean(values, -1, keepdims=True)
    spread = jnp.mean(center * center, -1, keepdims=True)
    normed = (center * lax.rsqrt(spread + NORM_EPS) * gain_ref[...]).astype(BF16)
    lane16 = iota((32, 16), 1)
    hit0 = routes_ref[:, 0:1] == lane16
    hit1 = routes_ref[:, 1:2] == lane16
    named = jnp.where(hit0 | hit1, 1.0, 0.0).astype(BF16)
    earlier = jnp.where(iota((32, 32), 1) < iota((32, 32), 0), 1.0, 0.0).astype(BF16)
    slot = mm(earlier, named).astype(BF16)
    expand = jnp.where((iota((256, 16), 0) >> 4) == iota((256, 16), 1), 1.0, 0.0).astype(BF16)
    r32 = iota((256, 32), 0)
    chosen = (nt(expand, named) > 0.5) & (nt(expand, slot) == (r32 & 7).astype(F32))
    first_half = ((r32 >> 3) & 1) == 0
    d0 = jnp.where(chosen & first_half, 1.0, 0.0).astype(BF16)
    d1 = jnp.where(chosen & jnp.logical_not(first_half), 1.0, 0.0).astype(BF16)
    packed = mm(d0, normed[:, : D // 2]) + mm(d1, normed[:, D // 2 :])
    asend[...] = packed.astype(BF16).reshape(EP, 16, D // 2)
    sksend[...] = jnp.broadcast_to(sink_ref[...], (8, 128))

    pl.semaphore_wait(barrier, 2 * (EP - 1))

    def a2a_send(j):
        to = wrap(e + j, EP)
        rcopy(asend.at[to], arecv.at[e], s_a.at[j], r_a.at[j], (to, t)).start()

    def a2a_wait(j):
        frm = wrap(e - j, EP)
        rcopy(asend.at[frm], arecv.at[frm], s_a.at[j], r_a.at[j], (frm, t)).wait_recv()

    each(1, EP, a2a_send)
    arecv[e] = asend[e]

    local[1].wait()

    def wz_copy(j):
        to = (e, wrap(z + j, NZ) * 2 + c)
        ref = wr.at[c, e, pl.ds(zrow, HEAD_DIM)]
        return rcopy(ref, ref, s_wz.at[j], r_wz.at[j], to)

    def wz_wait(j):
        frm = pl.multiple_of(wrap(z - j, NZ) * HEAD_DIM, HEAD_DIM)
        ref = wr.at[c, e, pl.ds(frm, HEAD_DIM)]
        rcopy(ref, ref, s_wz.at[j], r_wz.at[j], right).wait_recv()

    each(1, NZ, lambda j: wz_copy(j).start())

    local[0].wait()

    def pack(j):
        lo = qv[pl.ds(pl.multiple_of(j * 128, 128), 64), :]
        hi = qv[pl.ds(pl.multiple_of(j * 128 + 64, 64), 64), :]
        qsend[j] = jnp.concatenate([lo, hi], axis=1)

    each(0, TPN, pack)

    def q_send(j):
        to = wrap(t + j, TPN)
        rcopy(qsend.at[to], qrecv.at[t], s_q.at[j], r_q.at[j], (e, to)).start()
        rcopy(sksend, skrecv.at[t], s_k.at[j], r_k.at[j], (e, to)).start()

    def q_wait(j):
        frm = wrap(t - j, TPN)
        rcopy(qsend.at[frm], qrecv.at[frm], s_q.at[j], r_q.at[j], (e, frm)).wait_recv()
        rcopy(sksend, skrecv.at[frm], s_k.at[j], r_k.at[j], (e, frm)).wait_recv()

    each(1, TPN, q_send)
    qrecv[t] = qsend[t]
    skrecv[t] = sksend[...]
    after = (wrap(e + 1, EP), t)
    halo = [
        rcopy(k_hbm.at[pl.ds((TPN - 1) * WINDOW, WINDOW)], kbuf.at[2], s_h.at[0], r_h.at[0], after),
        rcopy(v_hbm.at[pl.ds((TPN - 1) * WINDOW, WINDOW)], vbuf.at[2], s_h.at[1], r_h.at[1], after),
    ]
    for cp in halo:
        cp.start()

    each(1, EP, a2a_wait)
    r96 = iota((ROWS, 256), 0)
    source = (r96 * 43) >> 8
    base = source * 16 + (r96 - source * CAP)
    arrived = arecv[...].reshape(256, D // 2)
    for h in range(2):
        pick = jnp.where(iota((ROWS, 256), 1) == base + h * 8, 1.0, 0.0).astype(BF16)
        agbuf[t, :, h * (D // 2) : (h + 1) * (D // 2)] = mm(pick, arrived).astype(BF16)

    def chip(direction, k):
        return wrap(z - k if direction == 0 else z + k, NZ)

    def block(zb, core, h):
        return agbuf.at[zb * 2 + core, pl.ds(h * HALF, HALF)]

    def ag_send(direction, k, h):
        ref = block(chip(direction, k - 1), c, h)
        return rcopy(
            ref,
            ref,
            s_ag.at[direction, k - 1, h],
            r_ag.at[direction, k - 1, h],
            ring[direction],
        )

    def ag_wait(direction, k, h):
        ref = block(chip(direction, k), c, h)
        rcopy(
            ref,
            ref,
            s_ag.at[direction, k - 1, h],
            r_ag.at[direction, k - 1, h],
            ring[direction],
        ).wait_recv()

    def d_send(slot_no, zb, h):
        ref = block(zb, c, h)
        return rcopy(ref, ref, s_d.at[slot_no, h], r_d.at[slot_no, h], partner)

    def d_wait(slot_no, zb, h):
        ref = block(zb, 1 - c, h)
        rcopy(ref, ref, s_d.at[slot_no, h], r_d.at[slot_no, h], partner).wait_recv()

    sends = []

    def go(copy):
        copy.start()
        sends.append(copy)

    for h in range(2):
        for direction in range(2):
            go(ag_send(direction, 1, h))
    for h in range(2):
        go(d_send(0, z, h))

    def x_copy(slot_no, zb):
        return rcopy(outbox.at[zb], inbox.at[zb], s_x.at[slot_no], r_x.at[slot_no], partner)

    def compute(zb, slot_no):
        x = jnp.concatenate([agbuf[zb * 2 + c], agbuf[zb * 2 + 1 - c]], axis=0)
        gate = mm(x, wg[...])
        up = mm(x, wu[...])
        hidden = (gate / (1.0 + jnp.exp(-gate)) * up).astype(BF16)
        for col in range(0, D, 512):
            part = mm(hidden, wd[:, col : col + 512])
            pbuf[zb, :, col : col + 512] = part[:ROWS]
            outbox[zb, :, col : col + 512] = part[ROWS:].astype(BF16)
        x_copy(slot_no, zb).start()

    def ring_step(k, h):
        for direction in range(2):
            if k <= LONG[direction][h]:
                ag_wait(direction, k, h)
                if k < LONG[direction][h]:
                    go(ag_send(direction, k + 1, h))
                go(d_send(direction * 4 + k, chip(direction, k), h))

    def event(k):
        for direction in range(2):
            for h in range(2):
                d_wait(direction * 4 + k, chip(direction, k), h)

        def one(i, carry):
            zb = wrap(z - k + 2 * k * i, NZ)
            compute(zb, i * 4 + k)
            return carry

        lax.fori_loop(0, 2, one, 0)

    for cp in local[6:]:
        cp.wait()
    for h in range(2):
        d_wait(0, z, h)
    compute(z, 0)
    each(1, NZ, wz_wait)

    def wp_copy(j):
        to = (wrap(e + j, EP), t)
        return rcopy(wr.at[c, e], wr.at[c, e], s_wp.at[j], r_wp.at[j], to)

    def wp_wait(j):
        frm = wrap(e - j, EP)
        rcopy(wr.at[c, frm], wr.at[c, frm], s_wp.at[j], r_wp.at[j], (frm, t)).wait_recv()

    each(1, EP, lambda j: wp_copy(j).start())

    def prepare_attention():
        for cp in local[2:6]:
            cp.wait()
        for cp in halo:
            cp.wait_recv()
        each(1, TPN, q_wait)
        low = iota((WINDOW, 128), 1) < HEAD_DIM
        for buf, out in ((kbuf, kz), (vbuf, vz)):
            for part in range(2):
                if part == 0:
                    full = jnp.where(t == 0, buf[2].astype(F32), buf[0].astype(F32))
                else:
                    full = buf[1].astype(F32)
                turned = pltpu.roll(full, HEAD_DIM, 1)
                at = pl.ds(part * WINDOW, WINDOW)
                out[0, 0, at] = jnp.where(low, full, 0.0).astype(BF16)
                out[0, 1, at] = jnp.where(low, 0.0, turned).astype(BF16)
                out[1, 0, at] = jnp.where(low, turned, 0.0).astype(BF16)
                out[1, 1, at] = jnp.where(low, 0.0, full).astype(BF16)

    def attend(j):
        core, pair = lax.rem(j, 2), j // 2
        group = j // 4
        token = iota((WINDOW, 2 * WINDOW), 0)
        key = iota((WINDOW, 2 * WINDOW), 1)
        begin = jnp.where((e == 0) & (t == 0), WINDOW, 0)
        allowed = (key > token) & (key <= token + WINDOW) & (key >= begin)
        total = None
        for i in range(2):
            head = pair * 4 + 2 * i + core
            q2 = qrecv[head]
            scores = jnp.concatenate([nt(q2, kz[group, 0]), nt(q2, kz[group, 1])], axis=0)
            masked = jnp.where(allowed, scores * HEAD_DIM**-0.5, -1e30)
            sink = skrecv[head][0:1, 0:1]
            row_max = jnp.maximum(jnp.max(masked, -1, keepdims=True), sink)
            powers = jnp.where(allowed, jnp.exp(masked - row_max), 0.0)
            sums = jnp.sum(powers, -1, keepdims=True) + jnp.exp(sink - row_max)
            probs = (powers / sums).astype(BF16)
            piece = mm(probs, vz[group, i])
            total = piece if total is None else total + piece
        att[j] = total.astype(BF16)

    ring_step(1, 0)
    prepare_attention()
    ring_step(1, 1)
    event(1)
    ring_step(2, 0)
    each(0, 4, attend)
    ring_step(2, 1)
    event(2)
    ring_step(3, 0)
    each(4, 8, attend)
    ring_step(3, 1)
    event(3)

    def x_wait(slot_no, zb):
        x_copy(slot_no, zb).wait_recv()

    def pair_sum(zb, h):
        at = pl.ds(h * HALF, HALF)
        return pbuf[zb, at] + inbox[zb, at].astype(F32)

    def rs_copy(direction, k, h):
        return rcopy(
            rs_send.at[direction, k - 1, h],
            rs_recv.at[direction, k - 1, h],
            s_rs.at[direction, k - 1, h],
            r_rs.at[direction, k - 1, h],
            ring[direction],
        )

    def rs_go(direction, k, h):
        away = LONG[direction][h] + 1 - k
        value = pair_sum(wrap(z + away if direction == 0 else z - away, NZ), h)
        if k > 1:
            value = value + rs_recv[direction, k - 2, h].astype(F32)
        rs_send[direction, k - 1, h] = value.astype(BF16)
        go(rs_copy(direction, k, h))

    x_wait(0, z)
    for k in range(1, 4):
        for direction in range(2):
            x_wait(direction * 4 + k, chip(direction, k))
    rs_go(0, 1, 1)
    rs_go(1, 1, 0)

    ag_wait(0, 4, 0)
    go(d_send(4, chip(0, 4), 0))
    ag_wait(1, 4, 1)
    go(d_send(8, chip(1, 4), 1))
    d_wait(4, chip(0, 4), 0)
    d_wait(8, chip(1, 4), 1)
    compute(chip(0, 4), 4)
    x_wait(4, chip(0, 4))
    rs_go(0, 1, 0)
    rs_go(1, 1, 1)

    each(1, EP, wp_wait)
    wd_copy = rcopy(wr.at[c], wr.at[c], s_wd, r_wd, partner)
    wd_copy.start()

    def project(lo, hi):
        a0 = jnp.concatenate([att[2 * i] for i in range(4)], axis=1)
        a1 = jnp.concatenate([att[2 * i + 1] for i in range(4)], axis=1)
        for i in range(lo, hi):
            out = mm(a0, wr[0, i]) + mm(a1, wr[1, i])
            mix_ref[:, i * 128 : (i + 1) * 128] = out.astype(BF16)

    def rs_step(k):
        for first in (True, False):
            for direction in range(2):
                h = 1 - direction if first else direction
                long = LONG[direction][h]
                if k <= long:
                    rs_copy(direction, k, h).wait_recv()
                    if k < long:
                        rs_go(direction, k + 1, h)

    rs_step(1)
    rcopy(wr.at[1 - c], wr.at[1 - c], s_wd, r_wd, partner).wait_recv()
    project(0, 8)
    rs_step(2)
    project(8, 16)
    rs_step(3)
    rs_step(4)

    halves = []
    for h in range(2):
        value = pair_sum(z, h)
        for direction in range(2):
            value = value + rs_recv[direction, LONG[direction][h] - 1, h].astype(F32)
        halves.append(value.astype(BF16))
    final = jnp.concatenate(halves, axis=0)
    rr = iota((256, ROWS), 0)
    want = (rr >> 4) * CAP + (rr & 7)
    good = (iota((256, ROWS), 1) == want) & ((rr & 7) < CAP)
    low_half = ((rr >> 3) & 1) == 0
    e0 = jnp.where(good & low_half, 1.0, 0.0).astype(BF16)
    e1 = jnp.where(good & jnp.logical_not(low_half), 1.0, 0.0).astype(BF16)
    spread_out = mm(e0, final[:, : D // 2]) + mm(e1, final[:, D // 2 :])
    bsend[...] = spread_out.astype(BF16).reshape(EP, 16, D // 2)

    def b_send(j):
        to = wrap(e + j, EP)
        rcopy(bsend.at[to], brecv.at[e], s_b.at[j], r_b.at[j], (to, t)).start()

    def b_wait(j):
        frm = wrap(e - j, EP)
        rcopy(bsend.at[frm], brecv.at[frm], s_b.at[j], r_b.at[j], (frm, t)).wait_recv()

    each(1, EP, b_send)
    brecv[e] = bsend[e]

    weight = jnp.where(hit0, rw_ref[:, 0:1], 0.0) + jnp.where(hit1, rw_ref[:, 1:2], 0.0)
    w_hi = weight.astype(BF16)
    w_lo = (weight - w_hi.astype(F32)).astype(BF16)
    lane = iota((32, 256), 1)
    mine = (nt(named, expand) > 0.5) & (nt(slot, expand) == (lane & 7).astype(F32))
    first_lane = ((lane >> 3) & 1) == 0
    hi_all = nt(w_hi, expand)
    lo_all = nt(w_lo, expand)
    each(1, EP, b_wait)
    back = brecv[...].reshape(256, D // 2)
    for h in range(2):
        keep = mine & (first_lane if h == 0 else jnp.logical_not(first_lane))
        out = mm(jnp.where(keep, hi_all, 0.0).astype(BF16), back)
        out = out + mm(jnp.where(keep, lo_all, 0.0).astype(BF16), back)
        moe_ref[:, h * (D // 2) : (h + 1) * (D // 2)] = out.astype(BF16)

    def drain(j):
        rcopy(asend.at[j], arecv.at[j], s_a.at[j], r_a.at[j], right).wait_send()
        rcopy(bsend.at[j], brecv.at[j], s_b.at[j], r_b.at[j], right).wait_send()
        rcopy(qsend.at[j], qrecv.at[j], s_q.at[j], r_q.at[j], right).wait_send()
        rcopy(sksend, skrecv.at[j], s_k.at[j], r_k.at[j], right).wait_send()
        wp_copy(j).wait_send()

    each(1, EP, drain)
    each(1, NZ, lambda j: wz_copy(j).wait_send())
    for cp in halo:
        cp.wait_send()
    wd_copy.wait_send()
    for cp in sends:
        cp.wait_send()
    x_copy(0, z).wait_send()
    for k in range(1, 4):
        for direction in range(2):
            x_copy(direction * 4 + k, chip(direction, k)).wait_send()
    x_copy(4, chip(0, 4)).wait_send()


def body(
    queries,
    key_rows,
    value_rows,
    sink_logits,
    out_weight,
    moe_rows,
    moe_gain,
    routes,
    route_weight,
    gate_weight,
    up_weight,
    down_weight,
):
    vm = pl.BlockSpec(memory_space=pltpu.VMEM)
    hbm = pl.BlockSpec(memory_space=pl.ANY)
    dma = pltpu.SemaphoreType.DMA
    half = D // 2
    return pl.pallas_call(
        kernel,
        out_shape=(
            jax.ShapeDtypeStruct((WINDOW, D), BF16),
            jax.ShapeDtypeStruct((32, D), BF16),
        ),
        in_specs=[vm] * 5 + [hbm] * 7,
        out_specs=(vm, vm),
        scratch_shapes=[
            pltpu.VMEM((D, FF), BF16),
            pltpu.VMEM((D, FF), BF16),
            pltpu.VMEM((FF, D), BF16),
            pltpu.VMEM((TPN * WINDOW, HEAD_DIM), BF16),
            pltpu.VMEM((TPN, 64, 128), BF16),
            pltpu.VMEM((TPN, 64, 128), BF16),
            pltpu.VMEM((8, 128), F32),
            pltpu.VMEM((TPN, 8, 128), F32),
            pltpu.VMEM((3, WINDOW, 128), BF16),
            pltpu.VMEM((3, WINDOW, 128), BF16),
            pltpu.VMEM((2, 2, 2 * WINDOW, 128), BF16),
            pltpu.VMEM((2, 2, 2 * WINDOW, 128), BF16),
            pltpu.VMEM((8, WINDOW, 128), BF16),
            pltpu.VMEM((2, EP, NZ * HEAD_DIM, 128), BF16),
            pltpu.VMEM((EP, 16, half), BF16),
            pltpu.VMEM((EP, 16, half), BF16),
            pltpu.VMEM((TPN, ROWS, D), BF16),
            pltpu.VMEM((NZ, ROWS, D), F32),
            pltpu.VMEM((NZ, ROWS, D), BF16),
            pltpu.VMEM((NZ, ROWS, D), BF16),
            pltpu.VMEM((2, 4, 2, HALF, D), BF16),
            pltpu.VMEM((2, 4, 2, HALF, D), BF16),
            pltpu.VMEM((EP, 16, half), BF16),
            pltpu.VMEM((EP, 16, half), BF16),
            dma((9,)),
            dma((EP,)),
            dma((EP,)),
            dma((EP,)),
            dma((EP,)),
            dma((TPN,)),
            dma((TPN,)),
            dma((TPN,)),
            dma((TPN,)),
            dma((2,)),
            dma((2,)),
            dma((NZ,)),
            dma((NZ,)),
            dma((EP,)),
            dma((EP,)),
            dma,
            dma,
            dma((2, 4, 2)),
            dma((2, 4, 2)),
            dma((9, 2)),
            dma((9, 2)),
            dma((8,)),
            dma((8,)),
            dma((2, 4, 2)),
            dma((2, 4, 2)),
        ],
        compiler_params=pltpu.CompilerParams(
            collective_id=0, has_side_effects=True, vmem_limit_bytes=60 * 1024 * 1024
        ),
    )(
        moe_rows,
        moe_gain.reshape(1, D),
        routes,
        route_weight,
        sink_logits.reshape(1, 1),
        queries,
        key_rows,
        value_rows,
        out_weight,
        gate_weight,
        up_weight,
        down_weight,
    )


def solution(mesh):
    in_specs = (
        P("ep", "tp"),
        P("ep", None),
        P("ep", None),
        P("tp"),
        P("tp", None),
        P(("ep", "tp"), None),
        P(),
        P(("ep", "tp"), None),
        P(("ep", "tp"), None),
        P("ep", None, "tp"),
        P("ep", None, "tp"),
        P("ep", "tp", None),
    )
    out_specs = (P(("ep", "tp"), None), P(("ep", "tp"), None))
    return jax.shard_map(body, mesh=mesh, in_specs=in_specs, out_specs=out_specs, check_vma=False)
```

time: 235 us -> 114 us (0.49)
  waiting for transfers between devices: 131 us -> 0 us
  Pallas kernels: 0 us -> 96.5 us
  matrix products: 36.6 us -> 0 us
  blocking collectives: 17.8 us -> 0 us
  between operations: 16.6 us -> 1.29 us
  starting transfers between devices: 9.03 us -> 0 us
  other arithmetic: 5.48 us -> 0 us
  local copies, waits for them, and re-layouts: 17.6 us -> 14.5 us
    reduce_scatter x3 -> x0, waiting for transfers between devices: 104 us -> none  [the longest x1 63.1 us: experts(): lax.psum_scatter(jnp.dot(hidden, down_mat, preferred_element_type=jnp.flo...]
    pallas_call x0 -> x1, Pallas kernels: none -> 96.5 us  [body(): pl.pallas_call(kernel, out_shape=(jax.ShapeDtypeStruct((WINDOW, D), BF16)...]
    dot_general x7 -> x0, matrix products: 36.6 us -> none  [the longest x1 13.2 us: experts(): jnp.dot(hidden, down_mat, preferred_element_type=jnp.float32)]
    all_to_all x1 -> x0, blocking collectives: 17.8 us -> none  [experts(): lax.all_to_all(buffer, 'ep', split_axis=0, concat_axis=0, tiled=True)]
    all_gather x1 -> x0, waiting for transfers between devices: 17 us -> none  [experts(): shard_rows = lax.all_gather(flat_rows, TP, axis=0, tiled=True)]
    unnamed x11 -> x9, local copies, waits for them, and re-layouts: 0.92 us -> 14.5 us
    all_to_all x1 -> x0, waiting for transfers between devices: 8.98 us -> none  [experts(): lax.all_to_all(results, 'ep', split_axis=0, concat_axis=0, tiled=True)]
    transpose x1 -> x0, local copies, waits for them, and re-layouts: 8.52 us -> none  [own_block(): blocks = jnp.moveaxis(blocks, order, range(len(axes))).reshape(-1, *inside)]
  transfers between devices with their start and end apart: 6 -> 0, of which waited for: 4 -> 0; matrix products, arithmetic and copies ran while one was open for 23% -> 0% of each run, Pallas kernels for 0% -> 0%
where the time goes in v1:
time: 114 us; the launch traced here: 112 us
  Pallas kernels  96.5 us (85%)
  local copies, waits for them, and re-layouts  14.5 us (13%)
  between operations  1.29 us (1%)
    pallas_call x1, Pallas kernels, body(): pl.pallas_call(kernel, out_shape=(jax.ShapeDtypeStruct((WINDOW, D), BF16)...  96.5 us
    unnamed x9, local copies, waits for them, and re-layouts  14.5 us

profile of v1, /device:TPU:1, one launch (start us, length us, event | category | flops | bytes accessed | tf_op | source)
XLA Modules:
  0.0 112.3 jit_solution(1592766757296800291)
XLA Ops:
  1.3 1.4 %copy.14.routes_ref = s32[32,2]{1,0:T(8,128)} copy(s32[32,2]{0,1:T(2,128)} %param.19) | data formatting | bytes 512 | tf_op args[7]
  2.6 1.4 %copy.15.rw_ref = f32[32,2]{1,0:T(8,128)} copy(f32[32,2]{0,1:T(2,128)} %param.20) | data formatting | bytes 512 | tf_op args[8]
  4.0 2.0 %copy.16.q_hbm = bf16[2048,64]{1,0:T(8,128)(2,1)} copy(bf16[2048,64]{0,1:T(8,128)(2,1)} %param.12) | data formatting | bytes 524288 | tf_op args[0]
  6.0 0.0 copy-start
  6.0 4.0 %copy.17.wg_hbm = bf16[1,2048,448]{2,1,0:T(8,128)(2,1)} copy(bf16[1,2048,448]{1,2,0:T(8,128)(2,1)} %param.21) | data formatting | bytes 3670016 | tf_op args[9]
  9.9 0.0 copy-done
  9.9 2.4 %copy.18.wu_hbm = bf16[1,2048,448]{2,1,0:T(8,128)(2,1)} copy(bf16[1,2048,448]{1,2,0:T(8,128)(2,1)S(1)} %copy-done) | data formatting | bytes 3670016 | tf_op args[10]
  12.3 96.5 %shard_map.131 = (bf16[128,2048]{1,0:T(8,128)(2,1)}, bf16[32,2048]{1,0:T(8,128)(2,1)}) custom-call(bf16[32,2048]{1,0:T(8,128)(2,1)} %rows_ref.1, f32[1,2048]{1,0:T(1,128)} %bitcast.3, s32[32,2]{1,0:T(8,128)} %copy.14.routes_ref, f32[32,2]{1,0:T(8,128)} %copy.15.rw_ref, f32[1,1]{1,0:T(1,128)} %bitcast.2.sink_ref, bf16[2048,64]{1,0:T(8,128)(2,1)} %copy.16.q_hbm, ...), custom_call_target="tpu_custom_call" | custom-call | tf_op jit(solution)/shard_map/pallas_call | solution.py:547
  108.9 1.9 %copy.22 = bf16[128,2048]{1,0:T(8,128)(2,1)} copy(bf16[128,2048]{1,0:T(8,128)(2,1)} %get-tuple-element.4) | data formatting | bytes 1048576
  110.8 1.6 %copy.23 = bf16[32,2048]{1,0:T(8,128)(2,1)} copy(bf16[32,2048]{1,0:T(8,128)(2,1)} %get-tuple-element.5) | data formatting | bytes 262144
Async XLA Ops:
  6.0 4.0 %copy-start = (bf16[1,2048,448]{1,2,0:T(8,128)(2,1)S(1)}, bf16[1,2048,448]{1,2,0:T(8,128)(2,1)}, u32[]{:S(2)}) copy-start(bf16[1,2048,448]{1,2,0:T(8,128)(2,1)} %param.22) | copy-start | bytes 5505028

commit v2 on v1

v2 whole, which is shorter than its diff:
```python
import jax
import jax.numpy as jnp
from jax import lax
from jax.experimental import pallas as pl
from jax.experimental.pallas import tpu as pltpu
from jax.sharding import PartitionSpec as P

MESH = pl.DeviceIdType.MESH
F32 = jnp.float32
BF16 = jnp.bfloat16
HEAD_DIM = 64
WINDOW = 128
NORM_EPS = 1e-5
EP = 16
NZ = 8
TPN = 16
ROWS = 96
HALF = 48
D = 2048
FF = 448
WIDE = D // 2
QUARTER = D // 4
NARROW = D // 2
LONG = ((4, 3), (3, 4))


def nt(a, b):
    return lax.dot_general(a, b, (((1,), (1,)), ((), ())), preferred_element_type=F32)


def mm(a, b):
    return jnp.dot(a, b, preferred_element_type=F32)


def iota(shape, dim):
    return lax.broadcasted_iota(jnp.int32, shape, dim)


def wrap(i, n):
    return lax.rem(i + n, n)


def kernel(
    rows_hbm,
    gain_hbm,
    routes_hbm,
    rw_hbm,
    sink_hbm,
    q_hbm,
    k_hbm,
    v_hbm,
    ow_hbm,
    wg_hbm,
    wu_hbm,
    wd_hbm,
    mix_ref,
    moe_ref,
    rows_ref,
    gain_ref,
    routes_ref,
    rw_ref,
    sink_ref,
    wg,
    wu,
    wd,
    qv,
    qz,
    sksend,
    skrecv,
    kbuf,
    vbuf,
    kf,
    vt,
    att,
    proj,
    wr,
    asend,
    arecv,
    agbuf,
    pbuf,
    outbox,
    inbox,
    rs_send,
    rs_recv,
    bsend,
    brecv,
    loc,
    q_sem,
    s_a,
    r_a,
    s_b,
    r_b,
    s_q,
    r_q,
    s_k,
    r_k,
    s_h,
    r_h,
    s_wz,
    r_wz,
    s_wp,
    r_wp,
    s_wd,
    r_wd,
    s_ag,
    r_ag,
    s_o,
    r_o,
    s_d,
    r_d,
    s_x,
    r_x,
    s_rs,
    r_rs,
):
    e = lax.axis_index("ep")
    t = lax.axis_index("tp")
    z = t // 2
    c = lax.rem(t, 2)
    right = (e, wrap(z + 1, NZ) * 2 + c)
    left = (e, wrap(z - 1, NZ) * 2 + c)
    partner = (e, z * 2 + 1 - c)
    ring = (right, left)

    def rcopy(src, dst, ss, rs, dev):
        return pltpu.make_async_remote_copy(
            src_ref=src, dst_ref=dst, send_sem=ss, recv_sem=rs, device_id=dev, device_id_type=MESH
        )

    def each(lo, hi, fn):
        def body(j, carry):
            fn(j)
            return carry

        lax.fori_loop(lo, hi, body, 0)

    first = [
        pltpu.make_async_copy(src, dst, loc.at[9 + i])
        for i, (src, dst) in enumerate(
            (
                (rows_hbm, rows_ref),
                (gain_hbm, gain_ref),
                (routes_hbm, routes_ref),
                (rw_hbm, rw_ref),
                (sink_hbm, sink_ref),
            )
        )
    ]
    for cp in first:
        cp.start()

    barrier = pltpu.get_barrier_semaphore()

    def greet(j):
        pl.semaphore_signal(barrier, inc=1, device_id=(wrap(e + j, EP), t), device_id_type=MESH)
        pl.semaphore_signal(barrier, inc=1, device_id=(e, wrap(t + j, TPN)), device_id_type=MESH)

    each(1, EP, greet)

    prev = jnp.maximum(t - 1, 0) * WINDOW
    prev = pl.multiple_of(prev, WINDOW)
    own = pl.multiple_of(t * WINDOW, WINDOW)
    wcol = pl.multiple_of(e * 128, 128)
    zrow = pl.multiple_of(z * HEAD_DIM, HEAD_DIM)
    group_row = pl.multiple_of((t // 8) * HEAD_DIM, HEAD_DIM)
    local = [
        pltpu.make_async_copy(
            q_hbm.at[:, pl.ds(own, WINDOW)],
            qz.at[t, pl.ds(group_row, HEAD_DIM)],
            loc.at[0],
        ),
        pltpu.make_async_copy(
            ow_hbm.at[:, pl.ds(wcol, 128)], wr.at[c, e, pl.ds(zrow, HEAD_DIM)], loc.at[1]
        ),
        pltpu.make_async_copy(k_hbm.at[pl.ds(prev, WINDOW)], kbuf.at[0], loc.at[2]),
        pltpu.make_async_copy(k_hbm.at[pl.ds(own, WINDOW)], kbuf.at[1], loc.at[3]),
        pltpu.make_async_copy(v_hbm.at[pl.ds(prev, WINDOW)], vbuf.at[0], loc.at[4]),
        pltpu.make_async_copy(v_hbm.at[pl.ds(own, WINDOW)], vbuf.at[1], loc.at[5]),
        pltpu.make_async_copy(wg_hbm.at[0], wg, loc.at[6]),
        pltpu.make_async_copy(wu_hbm.at[0], wu, loc.at[7]),
        pltpu.make_async_copy(wd_hbm.at[0], wd, loc.at[8]),
    ]
    for cp in local:
        cp.start()

    def q_load(j):
        cols = pl.ds(pl.multiple_of(j * WINDOW, WINDOW), WINDOW)
        pltpu.make_async_copy(q_hbm.at[:, cols], qv.at[j], q_sem).start()

    each(0, TPN, q_load)

    for cp in first:
        cp.wait()
    values = rows_ref[...].astype(F32)
    center = values - jnp.mean(values, -1, keepdims=True)
    spread = jnp.mean(center * center, -1, keepdims=True)
    normed = (center * lax.rsqrt(spread + NORM_EPS) * gain_ref[...]).astype(BF16)
    expert = iota((16, 32), 0)
    hit0 = routes_ref[0:1, :] == expert
    hit1 = routes_ref[1:2, :] == expert
    named = jnp.where(hit0 | hit1, 1.0, 0.0).astype(BF16)
    earlier = jnp.where(iota((32, 32), 0) < iota((32, 32), 1), 1.0, 0.0).astype(BF16)
    slot = mm(named, earlier).astype(BF16)
    expand = jnp.where((iota((256, 16), 0) >> 4) == iota((256, 16), 1), 1.0, 0.0).astype(BF16)
    r32 = iota((256, 32), 0)
    s32 = r32 & 3
    q32 = (r32 >> 2) & 3
    named_rows = mm(expand, named) > 0.5
    slot_rows = mm(expand, slot)
    chosen = []
    for h in range(2):
        chosen.append(named_rows & (s32 < 3) & (slot_rows == (s32 + 3 * h).astype(F32)))
        packed = None
        for q in range(4):
            take = jnp.where(chosen[h] & (q32 == q), 1.0, 0.0).astype(BF16)
            piece = mm(take, normed[:, q * QUARTER : (q + 1) * QUARTER])
            packed = piece if packed is None else packed + piece
        asend[h] = packed.astype(BF16).reshape(EP, 16, QUARTER)
    sksend[...] = jnp.broadcast_to(sink_ref[...], (8, 128))
    for head in range(TPN):
        unused = (1 - head // 8) * HEAD_DIM
        qz[head, unused : unused + HEAD_DIM] = jnp.zeros((HEAD_DIM, WINDOW), BF16)

    pl.semaphore_wait(barrier, 2 * (EP - 1))

    def a_copy(h, to, frm):
        return rcopy(asend.at[h, to], arecv.at[h, frm], s_a.at[h], r_a.at[h], (to, t))

    def a_send(h, j):
        to = wrap(e + j, EP)
        a_copy(h, to, e).start()

    def a_all(h):
        rest = slice(0, EP - 1)
        return rcopy(asend.at[h, rest], arecv.at[h, rest], s_a.at[h], r_a.at[h], right)

    for h in range(2):
        each(1, EP, lambda j: a_send(h, j))
    for h in range(2):
        arecv[h, e] = asend[h, e]

    local[1].wait()

    def wz_copy(direction, k):
        zb = wrap(z - k + 1 if direction == 0 else z + k - 1, NZ)
        ref = wr.at[c, e, pl.ds(pl.multiple_of(zb * HEAD_DIM, HEAD_DIM), HEAD_DIM)]
        return rcopy(ref, ref, s_wz, r_wz.at[direction, k - 1], ring[direction])

    def wz_step(k):
        for direction in range(2):
            if k <= 4 - direction:
                zb = wrap(z - k if direction == 0 else z + k, NZ)
                ref = wr.at[c, e, pl.ds(pl.multiple_of(zb * HEAD_DIM, HEAD_DIM), HEAD_DIM)]
                rcopy(ref, ref, s_wz, r_wz.at[direction, k - 1], right).wait_recv()
                if k < 4 - direction:
                    wz_copy(direction, k + 1).start()

    for direction in range(2):
        wz_copy(direction, 1).start()

    def q_copy(to, frm):
        rows = pl.ds(pl.multiple_of((frm // 8) * HEAD_DIM, HEAD_DIM), HEAD_DIM)
        return rcopy(qv.at[to], qz.at[frm, rows], s_q, r_q, (e, to))

    def q_send(j):
        to = wrap(t + j, TPN)
        q_copy(to, t).start()
        rcopy(sksend, skrecv.at[t], s_k, r_k, (e, to)).start()

    def q_all():
        ref = qz.at[pl.ds(0, TPN - 1), pl.ds(0, HEAD_DIM)]
        return rcopy(ref, ref, s_q, r_q, right)

    def k_all():
        ref = skrecv.at[pl.ds(0, TPN - 1)]
        return rcopy(ref, ref, s_k, r_k, right)

    pltpu.make_async_copy(qv, qv, q_sem).wait()
    each(1, TPN, q_send)
    skrecv[t] = sksend[...]
    after = (wrap(e + 1, EP), t)
    halo = [
        rcopy(k_hbm.at[pl.ds((TPN - 1) * WINDOW, WINDOW)], kbuf.at[2], s_h.at[0], r_h.at[0], after),
        rcopy(v_hbm.at[pl.ds((TPN - 1) * WINDOW, WINDOW)], vbuf.at[2], s_h.at[1], r_h.at[1], after),
    ]
    for cp in halo:
        cp.start()

    def compact(h):
        r48 = iota((HALF, 256), 0)
        source = (r48 * 43) >> 7
        base = source * 16 + (r48 - source * 3)
        lane = iota((HALF, 256), 1)
        arrived = arecv[h].reshape(256, QUARTER)
        for q in range(4):
            pick = jnp.where(lane == base + q * 4, 1.0, 0.0).astype(BF16)
            agbuf[t, h * HALF : (h + 1) * HALF, q * QUARTER : (q + 1) * QUARTER] = mm(
                pick, arrived
            ).astype(BF16)

    def chip(direction, k):
        return wrap(z - k if direction == 0 else z + k, NZ)

    def half_block(zb, core, h):
        return agbuf.at[zb * 2 + core, pl.ds(h * HALF, HALF)]

    def piece_of(zb, core, h, col):
        cols = pl.ds(0, NARROW) if col == 0 else pl.ds(NARROW, D - NARROW)
        return agbuf.at[zb * 2 + core, pl.ds(h * HALF, HALF), cols]

    def ag_copy(direction, k, h, col, zb):
        ref = piece_of(zb, c, h, col)
        return rcopy(
            ref,
            ref,
            s_ag,
            r_ag.at[direction, k - 1, h, col],
            ring[direction],
        )

    def d_copy(direction, k, h, col, core):
        ref = piece_of(chip(direction, k), core, h, col)
        return rcopy(
            ref,
            ref,
            s_d,
            r_d.at[direction, k - 1, h, col],
            partner,
        )

    def o_copy(h, core):
        ref = half_block(z, core, h)
        return rcopy(ref, ref, s_o, r_o.at[h], partner)

    def launch(h):
        a_all(h).wait_recv()
        compact(h)
        for col in range(2):
            for direction in range(2):
                ag_copy(direction, 1, h, col, z).start()
        o_copy(h, c).start()

    def x_copy(zb, h):
        at = pl.ds(h * HALF, HALF)
        return rcopy(outbox.at[zb, at], inbox.at[zb, at], s_x, r_x.at[zb, h], partner)

    def compute(parts):
        ats = [slice(h * HALF, (h + 1) * HALF) for _, h in parts]
        x = jnp.concatenate(
            [agbuf[zb * 2 + core, at] for core in (c, 1 - c) for (zb, _), at in zip(parts, ats)],
            axis=0,
        )
        gate = nt(x, wg[...])
        up = nt(x, wu[...])
        hidden = (gate / (1.0 + jnp.exp(-gate)) * up).astype(BF16)
        for col in range(0, D, 512):
            part = mm(hidden, wd[:, col : col + 512])
            for i, ((zb, _), at) in enumerate(zip(parts, ats)):
                other = (len(parts) + i) * HALF
                pbuf[zb, at, col : col + 512] = part[i * HALF : (i + 1) * HALF]
                outbox[zb, at, col : col + 512] = part[other : other + HALF].astype(BF16)
        for zb, h in parts:
            x_copy(zb, h).start()

    def arrival(k, h, long):
        for direction in range(2):
            col = direction if long else 1 - direction
            ag_copy(direction, k, h, col, chip(direction, k)).wait_recv()
            if k < LONG[direction][col]:
                ag_copy(direction, k + 1, h, col, chip(direction, k)).start()
            d_copy(direction, k, h, col, c).start()

    def event_wait(k, h):
        for col in range(2):
            for direction in range(2):
                if k <= LONG[direction][col]:
                    d_copy(direction, k, h, col, 1 - c).wait_recv()

    def event(k, h):
        if k == 0:
            o_copy(h, 1 - c).wait_recv()
            compute([(z, h)])
        else:
            event_wait(k, h)
            compute([(chip(0, k), h), (chip(1, k), h)] if k < 4 else [(chip(0, 4), h)])

    def wp_copy(j):
        to = (wrap(e + j, EP), t)
        return rcopy(wr.at[c, e], wr.at[c, e], s_wp, r_wp, to)

    def wp_all():
        ref = wr.at[c, pl.ds(0, EP - 1)]
        return rcopy(ref, ref, s_wp, r_wp, right)

    def prepare_attention():
        for cp in local[2:6]:
            cp.wait()
        for cp in halo:
            cp.wait_recv()
        q_all().wait_recv()
        k_all().wait_recv()
        local[0].wait()
        kf[:WINDOW] = jnp.where(t == 0, kbuf[2], kbuf[0])
        kf[WINDOW:] = kbuf[1]
        before = jnp.where(t == 0, vbuf[2], vbuf[0]).astype(F32)
        vt[:, :WINDOW] = before.T.astype(BF16)
        vt[:, WINDOW:] = vbuf[1].astype(F32).T.astype(BF16)

    def attend(head):
        token = iota((2 * WINDOW, WINDOW), 1)
        key = iota((2 * WINDOW, WINDOW), 0)
        begin = jnp.where((e == 0) & (t == 0), WINDOW, 0)
        allowed = (key > token) & (key <= token + WINDOW) & (key >= begin)
        scores = mm(kf[...], qz[head]) * HEAD_DIM**-0.5
        masked = jnp.where(allowed, scores, -1e30)
        sink = skrecv[head][0:1, :]
        row_max = jnp.maximum(jnp.max(masked, 0, keepdims=True), sink)
        powers = jnp.where(allowed, jnp.exp(masked - row_max), 0.0)
        sums = jnp.sum(powers, 0, keepdims=True) + jnp.exp(sink - row_max)
        probs = (powers / sums).astype(BF16)
        group = pl.multiple_of((head // 8) * HEAD_DIM, HEAD_DIM)
        place = pl.multiple_of((head // 2) * HEAD_DIM, HEAD_DIM)
        att[lax.rem(head, 2), pl.ds(place, HEAD_DIM)] = mm(vt[pl.ds(group, HEAD_DIM)], probs)

    def turn():
        for i in range(2):
            proj[i] = att[i].T.astype(BF16)

    def x_wait(zb, h):
        x_copy(zb, h).wait_recv()

    def pair_sum(zb, h, col):
        at = pl.ds(h * HALF, HALF)
        cols = slice(col * WIDE, (col + 1) * WIDE)
        return pbuf[zb, at, cols] + inbox[zb, at, cols].astype(F32)

    def rs_copy(direction, k, h, col):
        return rcopy(
            rs_send.at[direction, k - 1, h, col],
            rs_recv.at[direction, k - 1, h, col],
            s_rs,
            r_rs.at[direction, k - 1, h, col],
            ring[direction],
        )

    def rs_go(direction, k, h, col):
        away = LONG[direction][col] + 1 - k
        value = pair_sum(wrap(z + away if direction == 0 else z - away, NZ), h, col)
        if k > 1:
            value = value + rs_recv[direction, k - 2, h, col].astype(F32)
        rs_send[direction, k - 1, h, col] = value.astype(BF16)
        rs_copy(direction, k, h, col).start()

    def rs_begin(h, long):
        for direction in range(2):
            rs_go(direction, 1, h, direction if long else 1 - direction)

    def x_waits(k, h):
        x_wait(chip(0, k), h)
        if 0 < k < 4:
            x_wait(chip(1, k), h)

    def project(lo, hi):
        for i in range(lo, hi):
            out = mm(proj[0], wr[0, i]) + mm(proj[1], wr[1, i])
            mix_ref[:, i * 128 : (i + 1) * 128] = out.astype(BF16)

    def rs_step(k, h, long):
        for direction in range(2):
            col = direction if long else 1 - direction
            if k <= LONG[direction][col]:
                rs_copy(direction, k, h, col).wait_recv()
                if k < LONG[direction][col]:
                    rs_go(direction, k + 1, h, col)

    def b_copy(h, to, frm):
        return rcopy(bsend.at[h, to], brecv.at[h, frm], s_b.at[h], r_b.at[h], (to, t))

    def b_send(h, j):
        b_copy(h, wrap(e + j, EP), e).start()

    def b_all(h):
        rest = slice(0, EP - 1)
        return rcopy(bsend.at[h, rest], brecv.at[h, rest], s_b.at[h], r_b.at[h], right)

    def give_back(h):
        rr = iota((256, HALF), 0)
        good = (iota((256, HALF), 1) == (rr >> 4) * 3 + (rr & 3)) & ((rr & 3) < 3)
        spread_out = None
        for q in range(4):
            col, inner = q // 2, (q % 2) * QUARTER
            value = pair_sum(z, h, col)[:, inner : inner + QUARTER]
            for direction in range(2):
                last = LONG[direction][col] - 1
                value = value + rs_recv[direction, last, h, col, :, inner : inner + QUARTER].astype(F32)
            put = jnp.where(good & (((rr >> 2) & 3) == q), 1.0, 0.0).astype(BF16)
            piece = mm(put, value.astype(BF16))
            spread_out = piece if spread_out is None else spread_out + piece
        bsend[h] = spread_out.astype(BF16).reshape(EP, 16, QUARTER)
        each(1, EP, lambda j: b_send(h, j))
        brecv[h, e] = bsend[h, e]

    wz_step(1)
    launch(0)
    for cp in local[6:]:
        cp.wait()
    event(0, 0)
    launch(1)
    wz_step(2)
    prepare_attention()
    event(0, 1)
    arrival(1, 0, True)
    arrival(1, 0, False)
    arrival(1, 1, True)
    wz_step(3)
    each(0, 4, attend)
    arrival(2, 0, True)
    event(1, 0)
    arrival(2, 0, False)
    arrival(2, 1, True)
    event(2, 0)
    arrival(3, 0, True)
    wz_step(4)
    each(1, EP, lambda j: wp_copy(j).start())
    arrival(3, 0, False)
    arrival(1, 1, False)
    event(3, 0)
    arrival(3, 1, True)
    arrival(4, 0, True)
    each(4, 7, attend)
    x_waits(3, 0)
    rs_begin(0, False)
    arrival(2, 1, False)
    event(4, 0)
    arrival(4, 1, True)
    x_waits(4, 0)
    rs_begin(0, True)
    event(4, 1)
    x_waits(2, 0)
    rs_step(1, 0, False)
    arrival(3, 1, False)
    x_waits(4, 1)
    rs_begin(1, True)
    event(2, 1)
    rs_step(1, 0, True)
    each(7, 10, attend)
    x_waits(1, 0)
    rs_step(2, 0, False)
    event(3, 1)
    x_waits(3, 1)
    rs_step(1, 1, True)
    rs_step(2, 0, True)
    rs_begin(1, False)
    x_waits(2, 1)
    rs_step(2, 1, True)
    each(10, 13, attend)
    rs_step(3, 0, False)
    rs_step(3, 0, True)
    event(1, 1)
    rs_step(1, 1, False)
    x_waits(1, 1)
    rs_step(3, 1, True)
    each(13, 16, attend)
    turn()
    rs_step(4, 0, True)
    x_waits(0, 0)
    wp_all().wait_recv()
    wd_copy = rcopy(wr.at[c], wr.at[c], s_wd, r_wd, partner)
    wd_copy.start()
    give_back(0)
    rs_step(2, 1, False)
    rs_step(4, 1, True)
    rs_step(3, 1, False)
    x_waits(0, 1)
    give_back(1)
    rcopy(wr.at[1 - c], wr.at[1 - c], s_wd, r_wd, partner).wait_recv()
    project(0, 8)
    project(8, 16)

    weight = jnp.where(hit0, rw_ref[0:1, :], 0.0) + jnp.where(hit1, rw_ref[1:2, :], 0.0)
    w_hi = weight.astype(BF16)
    w_lo = (weight - w_hi.astype(F32)).astype(BF16)
    same = jnp.where(iota((32, 32), 0) == iota((32, 32), 1), 1.0, 0.0).astype(BF16)
    parts = [nt(same, mm(expand, part).astype(BF16)) for part in (w_hi, w_lo)]
    quarter = (iota((32, 256), 1) >> 2) & 3
    keep = [nt(same, jnp.where(chosen[h], 1.0, 0.0).astype(BF16)) > 0.5 for h in range(2)]
    for h in range(2):
        b_all(h).wait_recv()
    for q in range(4):
        out = None
        for h in range(2):
            back = brecv[h].reshape(256, QUARTER)
            for part in parts:
                piece = mm(jnp.where(keep[h] & (quarter == q), part, 0.0).astype(BF16), back)
                out = piece if out is None else out + piece
        moe_ref[:, q * QUARTER : (q + 1) * QUARTER] = out.astype(BF16)

    for h in range(2):
        a_all(h).wait_send()
        b_all(h).wait_send()
    q_all().wait_send()
    k_all().wait_send()
    wp_all().wait_send()
    seven = wr.at[c, e, pl.ds(0, (NZ - 1) * HEAD_DIM)]
    rcopy(seven, seven, s_wz, r_wp, right).wait_send()
    for cp in halo:
        cp.wait_send()
    wd_copy.wait_send()
    ring_bytes = agbuf.at[pl.ds(0, 7)]
    for sem in (s_ag, s_d, s_rs):
        rcopy(ring_bytes, ring_bytes, sem, r_wp, right).wait_send()
    rcopy(agbuf.at[t], agbuf.at[t], s_o, r_wp, partner).wait_send()
    rcopy(outbox, inbox, s_x, r_wp, partner).wait_send()


def hand_over(mixed, moved, mix_out, moe_out):
    mix_out[...] = mixed[...]
    moe_out[...] = moved[...]


def body(
    queries,
    key_rows,
    value_rows,
    sink_logits,
    out_weight,
    moe_rows,
    moe_gain,
    routes,
    route_weight,
    gate_weight,
    up_weight,
    down_weight,
):
    vm = pl.BlockSpec(memory_space=pltpu.VMEM)
    hbm = pl.BlockSpec(memory_space=pl.ANY)
    dma = pltpu.SemaphoreType.DMA
    mixed, moved = pl.pallas_call(
        kernel,
        out_shape=(
            jax.ShapeDtypeStruct((WINDOW, D), BF16),
            jax.ShapeDtypeStruct((32, D), BF16),
        ),
        in_specs=[hbm] * 12,
        out_specs=(vm, vm),
        scratch_shapes=[
            pltpu.VMEM((32, D), BF16),
            pltpu.VMEM((1, D), F32),
            pltpu.VMEM((2, 32), jnp.int32),
            pltpu.VMEM((2, 32), F32),
            pltpu.VMEM((1, 1), F32),
            pltpu.VMEM((FF, D), BF16),
            pltpu.VMEM((FF, D), BF16),
            pltpu.VMEM((FF, D), BF16),
            pltpu.VMEM((TPN, HEAD_DIM, WINDOW), BF16),
            pltpu.VMEM((TPN, 2 * HEAD_DIM, WINDOW), BF16),
            pltpu.VMEM((8, 128), F32),
            pltpu.VMEM((TPN, 8, 128), F32),
            pltpu.VMEM((3, WINDOW, 128), BF16),
            pltpu.VMEM((3, WINDOW, 128), BF16),
            pltpu.VMEM((2 * WINDOW, 128), BF16),
            pltpu.VMEM((128, 2 * WINDOW), BF16),
            pltpu.VMEM((2, NZ * HEAD_DIM, WINDOW), F32),
            pltpu.VMEM((2, WINDOW, NZ * HEAD_DIM), BF16),
            pltpu.VMEM((2, EP, NZ * HEAD_DIM, 128), BF16),
            pltpu.VMEM((2, EP, 16, QUARTER), BF16),
            pltpu.VMEM((2, EP, 16, QUARTER), BF16),
            pltpu.VMEM((TPN, ROWS, D), BF16),
            pltpu.VMEM((NZ, ROWS, D), F32),
            pltpu.VMEM((NZ, ROWS, D), BF16),
            pltpu.VMEM((NZ, ROWS, D), BF16),
            pltpu.VMEM((2, 4, 2, 2, HALF, WIDE), BF16),
            pltpu.VMEM((2, 4, 2, 2, HALF, WIDE), BF16),
            pltpu.VMEM((2, EP, 16, QUARTER), BF16),
            pltpu.VMEM((2, EP, 16, QUARTER), BF16),
            dma((14,)),
            dma,
            dma((2,)),
            dma((2,)),
            dma((2,)),
            dma((2,)),
            dma,
            dma,
            dma,
            dma,
            dma((2,)),
            dma((2,)),
            dma,
            dma((2, 4)),
            dma,
            dma,
            dma,
            dma,
            dma,
            dma((2, 4, 2, 2)),
            dma,
            dma((2,)),
            dma,
            dma((2, 4, 2, 2)),
            dma,
            dma((NZ, 2)),
            dma,
            dma((2, 4, 2, 2)),
        ],
        compiler_params=pltpu.CompilerParams(
            collective_id=0, has_side_effects=True, vmem_limit_bytes=60 * 1024 * 1024
        ),
    )(
        moe_rows,
        moe_gain.reshape(1, D),
        routes.T,
        route_weight.T,
        sink_logits.reshape(1, 1),
        queries.T,
        key_rows,
        value_rows,
        out_weight,
        jnp.swapaxes(gate_weight, 1, 2),
        jnp.swapaxes(up_weight, 1, 2),
        down_weight,
    )
    return pl.pallas_call(
        hand_over,
        out_shape=(
            jax.ShapeDtypeStruct((WINDOW, D), BF16),
            jax.ShapeDtypeStruct((32, D), BF16),
        ),
        in_specs=[vm, vm],
        out_specs=(vm, vm),
    )(mixed, moved)


def solution(mesh):
    in_specs = (
        P("ep", "tp"),
        P("ep", None),
        P("ep", None),
        P("tp"),
        P("tp", None),
        P(("ep", "tp"), None),
        P(),
        P(("ep", "tp"), None),
        P(("ep", "tp"), None),
        P("ep", None, "tp"),
        P("ep", None, "tp"),
        P("ep", "tp", None),
    )
    out_specs = (P(("ep", "tp"), None), P(("ep", "tp"), None))
    return jax.shard_map(body, mesh=mesh, in_specs=in_specs, out_specs=out_specs, check_vma=False)
```

time: 114 us -> 91.6 us (0.80); the launches traced: 112 us -> 91.3 us
  local copies, waits for them, and re-layouts: 14.5 us -> 0 us
  Pallas kernels: 96.5 us -> 90 us
    unnamed x9 -> x0, local copies, waits for them, and re-layouts: 14.5 us -> none
    pallas_call x1, Pallas kernels: 96.5 us -> 88.1 us  [body(): pl.pallas_call(kernel, out_shape=(jax.ShapeDtypeStruct((WINDOW, D), BF16)...]
    pallas_call x0 -> x1, Pallas kernels: none -> 1.93 us  [body(): pl.pallas_call(hand_over, out_shape=(jax.ShapeDtypeStruct((WINDOW, D), BF...]
where the time goes in v2:
time: 91.6 us; the launch traced here: 91.3 us
  Pallas kernels  90 us (98%)
  between operations  1.29 us (1%)
    pallas_call x1, Pallas kernels, body(): pl.pallas_call(kernel, out_shape=(jax.ShapeDtypeStruct((WINDOW, D), BF16)...  88.1 us
    pallas_call x1, Pallas kernels, body(): pl.pallas_call(hand_over, out_shape=(jax.ShapeDtypeStruct((WINDOW, D), BF...  1.93 us

profile of v2, /device:TPU:1, one launch (start us, length us, event | category | flops | bytes accessed | tf_op | source)
XLA Modules:
  0.0 91.3 jit_solution(17618945447386410587)
XLA Ops:
  1.3 88.1 %shard_map.131 = (bf16[128,2048]{1,0:T(8,128)(2,1)}, bf16[32,2048]{1,0:T(8,128)(2,1)}) custom-call(bf16[32,2048]{1,0:T(8,128)(2,1)} %rows_hbm.1, f32[1,2048]{1,0:T(1,128)} %bitcast.11, s32[2,32]{1,0:T(2,128)} %bitcast.12, f32[2,32]{1,0:T(2,128)} %bitcast.13, f32[1,1]{1,0:T(1,128)} %bitcast.7.sink_hbm, bf16[64,2048]{1,0:T(8,128)(2,1)} %bitcast.10, ...), custom_call_target="tpu_custom_call" | custom-call | tf_op jit(solution)/shard_map/pallas_call | solution.py:638
  89.4 1.9 %shard_map.132 = (bf16[128,2048]{1,0:T(8,128)(2,1)}, bf16[32,2048]{1,0:T(8,128)(2,1)}) custom-call(bf16[128,2048]{1,0:T(8,128)(2,1)} %get-tuple-element.4.mixed, bf16[32,2048]{1,0:T(8,128)(2,1)} %get-tuple-element.5.moved), custom_call_target="tpu_custom_call" | custom-call | tf_op jit(solution)/shard_map/pallas_call | solution.py:722
